TPU v7x, 1024 devices: a whole 4x4x32 slice. The times are simulated.
1024 devices in a mesh: ep: 64 (over z, core), tp: 16 (over y, x).
Axes of the slice: x: 4, y: 4, z: 32, core: 2. Of those that a mesh axis runs over, the one named last changes fastest.
Arguments:
- tokens: bfloat16 [4096, 2048], P('ep'), may hold values from -6 to 6
- mix_gain: float32 [2048], replicated, may hold values from 0.1 to 1.9
- w_in: bfloat16 [2048, 1024], P(None, 'tp'), may hold values from -0.125 to 0.125
- decay_re: float32 [64, 64], P('tp'), may hold values from -1 to -0.1
- freq: float32 [64, 64], P('tp'), may hold values from 0 to 100
- log_step: float32 [64], P('tp'), may hold values from -3.9 to 0
- in_re: bfloat16 [64, 16, 64], P('tp'), may hold values from -1 to 1
- in_im: bfloat16 [64, 16, 64], P('tp'), may hold values from -1 to 1
- out_re: bfloat16 [64, 16, 64], P('tp'), may hold values from -0.75 to 0.75
- out_im: bfloat16 [64, 16, 64], P('tp'), may hold values from -0.75 to 0.75
- skip: float32 [64, 16], P('tp'), may hold values from -4 to 4
- state_re: float32 [4096, 64, 64], P('ep', 'tp'), may hold values from -6 to 6
- state_im: float32 [4096, 64, 64], P('ep', 'tp'), may hold values from -6 to 6
- glu_weight: bfloat16 [1024, 1024], P(None, 'tp'), may hold values from -0.1875 to 0.1875
- glu_bias: float32 [1024], P('tp'), may hold values from -4 to 4
- out_weight: bfloat16 [1024, 2048], P('tp'), may hold values from -0.1875 to 0.1875
- ffn_gain: float32 [2048], replicated, may hold values from 0.1 to 1.9
- route: int32 [4096, 2], P('ep'), may hold values from 0 to 63, all different within a row; in each aligned block of 64 rows (0 to 63, 64 to 127, ...) at most 3 rows name the same one
- route_weight: float32 [4096, 2], P('ep'), may hold values from 0.2 to 1
- expert_gate: bfloat16 [64, 2048, 3584], P('ep', None, 'tp'), may hold values from -0.125 to 0.125
- expert_up: bfloat16 [64, 2048, 3584], P('ep', None, 'tp'), may hold values from -0.125 to 0.125
- expert_down: bfloat16 [64, 3584, 2048], P('ep', 'tp'), may hold values from -0.09375 to 0.09375
Outputs:
- mixed: bfloat16 [4096, 2048], P('ep', 'tp')
- new_re: float32 [4096, 64, 64], P('ep', 'tp')
- new_im: float32 [4096, 64, 64], P('ep', 'tp')
Inputs may be any that keep to these rules, and one draw needn't show every extreme that they name: `route`: each row names 2 different experts. Within the 64 rows of one index of ep no expert is named more than 3 times, and in every draw some expert is named exactly 3 times by the rows of some index of ep.
All inputs are finite; a program needn't handle non-finite values.
Results may differ from a plain program's by a relative error of at most 0.015.
Values may be sent and summed in bfloat16 or wider, within the bound.
A program may use at most 32 MiB of HBM per device.

v0:
```python
import functools

import jax
import jax.numpy as jnp
from jax import lax
from jax.sharding import Mesh
from jax.sharding import PartitionSpec as P

TP = ("tp_0", "tp_1")
EP = ("ep_0", "ep_1")


norm_eps = 1e-06


def in_order(parts, dim):
    dims = list(parts.shape[1:])
    dims[dim] *= parts.shape[0]
    return jnp.moveaxis(parts, 0, dim).reshape(dims)


def from_everyone(shard, axis):
    copies = jnp.broadcast_to(shard, (lax.axis_size(axis), *shard.shape))
    return lax.all_to_all(copies, axis, split_axis=0, concat_axis=0, tiled=True)


def gathered_copies(shard, axis, dim):
    return in_order(from_everyone(shard, axis), dim)


def split_up(shard, dim, size):
    dims = shard.shape
    parts = shard.reshape(*dims[:dim], size, dims[dim] // size, *dims[dim + 1 :])
    return jnp.moveaxis(parts, dim, 0)


def summed_on_arrival(shard, axis, dim):
    size = lax.axis_size(axis)
    parts = lax.all_to_all(split_up(shard, dim, size), axis, 0, 0, tiled=True)
    return jnp.sum(parts.astype(jnp.float32), axis=0)


def one_axis_at_a_time(shard, axes):
    return functools.reduce(lax.psum, axes, shard)


def turned_blocks(parts, axes, turns):
    dims = [lax.axis_size(a) for a in axes]
    parts = parts.reshape(*dims, *parts.shape[1:])
    for k in turns:
        parts = lax.all_to_all(parts, axes[k], split_axis=k, concat_axis=k, tiled=True)
    return parts.reshape(-1, *parts.shape[len(axes) :])


def core_and_chips(shard, groups, turns, split_dim, concat_dim):
    size = lax.axis_size(groups[0]) * lax.axis_size(groups[1])
    parts = split_up(shard, split_dim, size)
    return in_order(turned_blocks(parts, groups, turns), concat_dim)


def rms_scale(rows, gain):
    values = rows.astype(jnp.float32)
    scaled = values * lax.rsqrt(jnp.mean(values * values, axis=-1, keepdims=True) + norm_eps)
    return (scaled * gain).astype(jnp.bfloat16)


def state_step(
    inputs, state_re, state_im, decay_re, freq, log_step, in_re, in_im, out_re, out_im, skip
):
    highest = lax.Precision.HIGHEST
    step = jnp.exp(log_step)[:, None]
    magnitude = jnp.exp(decay_re * step)
    turn_re = magnitude * jnp.cos(freq * step)
    turn_im = magnitude * jnp.sin(freq * step)
    denom = decay_re * decay_re + freq * freq
    coef_re = ((turn_re - 1.0) * decay_re + turn_im * freq) / denom
    coef_im = (turn_im * decay_re - (turn_re - 1.0) * freq) / denom
    drive_re = jnp.einsum("sgh,ghp->sgp", inputs, in_re, preferred_element_type=jnp.float32)
    drive_im = jnp.einsum("sgh,ghp->sgp", inputs, in_im, preferred_element_type=jnp.float32)
    push_re = coef_re * drive_re - coef_im * drive_im
    push_im = coef_re * drive_im + coef_im * drive_re
    new_re = turn_re * state_re - turn_im * state_im + push_re
    new_im = turn_re * state_im + turn_im * state_re + push_im
    read = jnp.einsum("ghp,sgp->sgh", out_re.astype(jnp.float32), new_re, precision=highest)
    read = read - jnp.einsum("ghp,sgp->sgh", out_im.astype(jnp.float32), new_im, precision=highest)
    read = read + skip * inputs.astype(jnp.float32)
    return (read, new_re, new_im)


def local(
    tokens,
    mix_gain,
    w_in,
    decay_re,
    freq,
    log_step,
    in_re,
    in_im,
    out_re,
    out_im,
    skip,
    state_re,
    state_im,
    glu_weight,
    glu_bias,
    out_weight,
    ffn_gain,
    route,
    route_weight,
    expert_gate,
    expert_up,
    expert_down,
):
    seq_count = tokens.shape[0]
    groups_local = decay_re.shape[0]
    model_width = tokens.shape[1]
    local_width = model_width // lax.axis_size(TP)
    experts = lax.axis_size(EP)
    top_count = route.shape[1]
    slot_cap = (3 * seq_count * top_count + 2 * experts - 1) // (2 * experts)
    col_start = lax.axis_index(TP) * local_width
    normed = rms_scale(tokens, mix_gain)
    drive = jnp.dot(normed, w_in, preferred_element_type=jnp.float32).astype(jnp.bfloat16)
    inputs = drive.reshape(seq_count, groups_local, -1)
    read, new_re, new_im = state_step(
        inputs, state_re, state_im, decay_re, freq, log_step, in_re, in_im, out_re, out_im, skip
    )
    mixed_in = jax.nn.gelu(read).reshape(seq_count, -1).astype(jnp.bfloat16)
    gate = jnp.dot(gathered_copies(mixed_in, TP, 1), glu_weight, preferred_element_type=jnp.float32)
    gated = (mixed_in.astype(jnp.float32) * jax.nn.sigmoid(gate + glu_bias)).astype(jnp.bfloat16)
    partial_value = jnp.dot(gated, out_weight, preferred_element_type=jnp.float32)
    mix_part = summed_on_arrival(partial_value.astype(jnp.bfloat16), TP, 1)
    token_part = lax.dynamic_slice_in_dim(tokens, col_start, local_width, 1)
    resid_part = (token_part.astype(jnp.float32) + mix_part).astype(jnp.bfloat16)
    part_values = resid_part.astype(jnp.float32)
    squares = one_axis_at_a_time(jnp.sum(part_values * part_values, axis=1), TP)
    row_scale = lax.rsqrt(squares / model_width + norm_eps)
    gain_part = lax.dynamic_slice_in_dim(ffn_gain, col_start, local_width, 0)
    own_cols = (part_values * row_scale[:, None] * gain_part).astype(jnp.bfloat16)
    flat_route = route.reshape(-1)
    hits = (flat_route[:, None] == jnp.arange(experts)[None, :]).astype(jnp.int32)
    rank = jnp.sum((jnp.cumsum(hits, axis=0) - hits) * hits, axis=1)
    slot = flat_route * slot_cap + rank
    slot_ids = jnp.arange(experts * slot_cap)
    picks = (slot[None, :] == slot_ids[:, None]).reshape(experts * slot_cap, seq_count, top_count)
    select = jnp.any(picks, axis=2).astype(jnp.bfloat16)
    combine = jnp.einsum("ask,sk->sa", picks.astype(jnp.float32), route_weight)
    gate_local = expert_gate[0]
    up_local = expert_up[0]
    down_local = expert_down[0]
    outbound = jnp.dot(select, own_cols, preferred_element_type=jnp.float32).astype(jnp.bfloat16)
    arrived = core_and_chips(
        outbound.reshape(experts, slot_cap, local_width), ("ep_0", "ep_1"), (1, 0), 0, 0
    )
    piece = gathered_copies(arrived, TP, 2)
    rows_piece = piece.reshape(experts * slot_cap, piece.shape[2])
    gate_rows = jnp.dot(rows_piece, gate_local, preferred_element_type=jnp.float32)
    up_rows = jnp.dot(rows_piece, up_local, preferred_element_type=jnp.float32)
    hidden = (jax.nn.silu(gate_rows) * up_rows).astype(jnp.bfloat16)
    back_rows = summed_on_arrival(
        lax.dot_general(
            down_local, hidden, (((0,), (1,)), ((), ())), preferred_element_type=jnp.float32
        ).astype(jnp.bfloat16),
        TP,
        0,
    )
    back_rows = back_rows.astype(jnp.bfloat16).reshape(local_width, experts, slot_cap)
    returned = lax.all_to_all(back_rows, EP, split_axis=1, concat_axis=1, tiled=True)
    returned = returned.reshape(local_width, experts * slot_cap).astype(jnp.float32)
    expert_total = lax.dot_general(
        combine, returned, (((1,), (1,)), ((), ())), precision=lax.Precision.HIGHEST
    )
    mixed = (resid_part.astype(jnp.float32) + expert_total).astype(jnp.bfloat16)
    return (mixed, new_re, new_im)


def solution(mesh):
    split = Mesh(mesh.devices.reshape(32, 2, 4, 4), ("ep_0", "ep_1", "tp_0", "tp_1"))
    placed = (
        P(EP, None),
        P(),
        P(None, TP),
        P(TP, None),
        P(TP, None),
        P(TP),
        P(TP, None, None),
        P(TP, None, None),
        P(TP, None, None),
        P(TP, None, None),
        P(TP, None),
        P(EP, TP, None),
        P(EP, TP, None),
        P(None, TP),
        P(TP),
        P(TP, None),
        P(),
        P(EP, None),
        P(EP, None),
        P(EP, None, TP),
        P(EP, None, TP),
        P(EP, TP, None),
    )
    return jax.shard_map(
        local,
        mesh=split,
        in_specs=placed,
        out_specs=(P(EP, TP), P(EP, TP, None), P(EP, TP, None)),
        check_vma=False,
    )
```

profile of v0, /device:TPU:1, one launch (start us, length us, event | category | flops | bytes accessed | tf_op | source)
XLA Modules:
  0.0 179.3 jit_solution(11927679829285992148)
XLA Ops:
  0.7 0.7 exp.13
  1.5 1.1 fusion.23
  2.6 1.3 convolution_convert_fusion.3
  5.3 0.9 reshape.71
  6.2 7.6 %all-to-all-start = ((bf16[16,2,2048]{2,1,0:T(2,128)(2,1)}), bf16[16,2,2048]{2,1,0:T(2,128)(2,1)S(1)}, u32[]{:S(2)}, u32[]{:S(2)}) async-start(bf16[16,2,2048]{2,1,0:T(2,128)(2,1)} %reshape.71), calls=%async_computation | async-start | bytes 262144 | tf_op jit(solution)/shard_map/all_to_all | solution.py:24
  14.8 5.9 %all-to-all-done = bf16[16,2,2048]{2,1,0:T(2,128)(2,1)S(1)} async-done(((bf16[16,2,2048]{2,1,0:T(2,128)(2,1)}), bf16[16,2,2048]{2,1,0:T(2,128)(2,1)S(1)}, u32[]{:S(2)}, u32[]{:S(2)}) %all-to-all-start) | async-done | bytes 131104 | tf_op jit(solution)/shard_map/all_to_all | solution.py:24
  21.7 0.8 copy.172
  22.4 3.5 %all-to-all-start.1 = ((bf16[16,64,128]{2,1,0:T(8,128)(2,1)}), bf16[16,64,128]{2,1,0:T(8,128)(2,1)S(1)}, u32[]{:S(2)}, u32[]{:S(2)}) async-start(bf16[16,64,128]{2,1,0:T(8,128)(2,1)} %bitcast.71), calls=%async_computation.1 | async-start | bytes 524288 | tf_op jit(solution)/shard_map/all_to_all | solution.py:39
  26.0 0.8 dynamic_slice.7
  26.9 6.6 %all-to-all-done.1 = bf16[16,64,128]{2,1,0:T(8,128)(2,1)S(1)} async-done(((bf16[16,64,128]{2,1,0:T(8,128)(2,1)}), bf16[16,64,128]{2,1,0:T(8,128)(2,1)S(1)}, u32[]{:S(2)}, u32[]{:S(2)}) %all-to-all-start.1) | async-done | bytes 262176 | tf_op jit(solution)/shard_map/all_to_all | solution.py:39
  33.5 0.8 fusion.48
  34.4 6.5 %psum.14 = f32[64]{0:T(128)S(1)} all-reduce(f32[64]{0:T(128)S(1)} %get-tuple-element.24), channel_id=1, replica_groups=mesh['ep_0'=32,'ep_1'=2,'tp_0'=4,'tp_1'=4] {'tp_0'}, use_global_device_ids=true, to_apply=%region_6.7 | all-reduce | flops 64 | bytes 512 | tf_op jit(solution)/shard_map/psum | solution.py:44
  40.9 6.7 %psum.15 = f32[64]{0:T(128)S(1)} all-reduce(f32[64]{0:T(128)S(1)} %psum.14), channel_id=1, replica_groups=mesh['ep_0'=32,'ep_1'=2,'tp_0'=4,'tp_1'=4] {'tp_1'}, use_global_device_ids=true, to_apply=%region_7.8 | all-reduce | flops 64 | bytes 512 | tf_op jit(solution)/shard_map/psum | solution.py:44
  47.9 19.8 %all_to_all.35 = bf16[32,2,1,3,128]{4,0,3,2,1:T(8,128)(2,1)S(1)} all-to-all(bf16[32,2,1,3,128]{4,0,3,2,1:T(8,128)(2,1)S(1)} %copy.137), channel_id=1, replica_groups=mesh['ep_0'=32,'ep_1'=2,'tp_0'=4,'tp_1'=4] {'ep_1'}, dimensions={1} | all-to-all | bytes 98304 | tf_op jit(solution)/shard_map/all_to_all | solution.py:51
  67.7 42.4 %all_to_all.36 = bf16[32,2,1,3,128]{4,1,3,2,0:T(2,128)(2,1)S(1)} all-to-all(bf16[32,2,1,3,128]{4,1,3,2,0:T(2,128)(2,1)S(1)} %copy.138), channel_id=1, replica_groups=mesh['ep_0'=32,'ep_1'=2,'tp_0'=4,'tp_1'=4] {'ep_0'}, dimensions={0} | all-to-all | bytes 98304 | tf_op jit(solution)/shard_map/all_to_all | solution.py:51
  110.4 14.7 %all_to_all.37 = bf16[16,64,3,128]{3,1,2,0:T(8,128)(2,1)S(1)} all-to-all(bf16[16,64,3,128]{3,1,2,0:T(8,128)(2,1)S(1)} %broadcast_in_dim.5), channel_id=1, replica_groups=mesh['ep_0'=32,'ep_1'=2,'tp_0'=4,'tp_1'=4] {'tp_0','tp_1'}, dimensions={0} | all-to-all | bytes 1572864 | tf_op jit(solution)/shard_map/all_to_all | solution.py:24
  125.5 0.7 copy-done.15
  126.7 2.3 %fusion = bf16[24,16,8,128]{3,2,1,0:T(8,128)(2,1)S(1)} fusion(bf16[1,224,2048]{2,1,0:T(8,128)(2,1)S(1)} %copy-done, bf16[1,2048,224]{1,2,0:T(8,128)(2,1)} %param.42, bf16[24,8,16,128]{3,2,1,0:T(8,128)(2,1)S(1)} %bitcast.76, f32[192,224]{1,0:T(8,128)S(1)} %fusion.15), kind=kOutput, calls=%fused_computation.2 | convolution fusion | flops 352972800 | bytes 3579904 | tf_op jit(solution)/shard_map/dot_general | solution.py:161
  129.2 14.1 %all_to_all.38 = bf16[16,128,192]{1,2,0:T(8,128)(2,1)S(1)} all-to-all(bf16[16,128,192]{1,2,0:T(8,128)(2,1)S(1)} %bitcast.73), channel_id=1, replica_groups=mesh['ep_0'=32,'ep_1'=2,'tp_0'=4,'tp_1'=4] {'tp_0','tp_1'}, dimensions={0} | all-to-all | bytes 1572864 | tf_op jit(solution)/shard_map/all_to_all | solution.py:39
  144.1 9.3 %all-to-all-start.6 = ((bf16[128,64,3]{0,2,1:T(4,128)(2,1)}), bf16[128,64,3]{0,2,1:T(4,128)(2,1)S(1)}, u32[]{:S(2)}, u32[]{:S(2)}) async-start(bf16[128,64,3]{0,2,1:T(4,128)(2,1)} %reshape.67), calls=%async_computation.6 | async-start | bytes 131072 | tf_op jit(solution)/shard_map/all_to_all | solution.py:168
  153.3 0.7 copy.142
  154.1 0.7 copy.143
  155.2 23.3 %all-to-all-done.6 = bf16[128,64,3]{0,2,1:T(4,128)(2,1)S(1)} async-done(((bf16[128,64,3]{0,2,1:T(4,128)(2,1)}), bf16[128,64,3]{0,2,1:T(4,128)(2,1)S(1)}, u32[]{:S(2)}, u32[]{:S(2)}) %all-to-all-start.6) | async-done | bytes 49184 | tf_op jit(solution)/shard_map/all_to_all | solution.py:168
  178.5 0.8 fusion.10
  (69 shorter events, 6.2 us)
Async XLA Ops:
  0.6 126.0 %copy-start = (bf16[1,224,2048]{2,1,0:T(8,128)(2,1)S(1)}, bf16[1,224,2048]{2,1,0:T(8,128)(2,1)}, u32[]{:S(2)}) copy-start(bf16[1,224,2048]{2,1,0:T(8,128)(2,1)} %param.43) | copy-start | bytes 2752516
  0.6 3.4 %copy-start.5 = (bf16[4,16,64]{2,1,0:T(8,128)(2,1)S(1)}, bf16[4,16,64]{2,1,0:T(8,128)(2,1)}, u32[]{:S(2)}) copy-start(bf16[4,16,64]{2,1,0:T(8,128)(2,1)} %param.29) | copy-start | bytes 24580
  0.7 3.6 %copy-start.12 = (f32[4,64]{1,0:T(4,128)S(1)}, f32[4,64]{1,0:T(4,128)}, u32[]{:S(2)}) copy-start(f32[4,64]{1,0:T(4,128)} %param.25) | copy-start | bytes 3076
  0.7 3.6 %copy-start.11 = (f32[4,64]{1,0:T(4,128)S(1)}, f32[4,64]{1,0:T(4,128)}, u32[]{:S(2)}) copy-start(f32[4,64]{1,0:T(4,128)} %param.26) | copy-start | bytes 3076
  0.7 3.7 %copy-start.6 = (bf16[4,16,64]{2,1,0:T(8,128)(2,1)S(1)}, bf16[4,16,64]{2,1,0:T(8,128)(2,1)}, u32[]{:S(2)}) copy-start(bf16[4,16,64]{2,1,0:T(8,128)(2,1)} %param.28) | copy-start | bytes 24580
  0.7 3.7 %copy-start.3 = (f32[64,4,64]{2,1,0:T(4,128)S(1)}, f32[64,4,64]{2,1,0:T(4,128)}, u32[]{:S(2)}) copy-start(f32[64,4,64]{2,1,0:T(4,128)} %param.33) | copy-start | bytes 196612
  0.7 3.7 %copy-start.2 = (f32[64,4,64]{2,1,0:T(4,128)S(1)}, f32[64,4,64]{2,1,0:T(4,128)}, u32[]{:S(2)}) copy-start(f32[64,4,64]{2,1,0:T(4,128)} %param.34) | copy-start | bytes 196612
  1.5 3.2 %copy-start.7 = (bf16[4,16,64]{2,1,0:T(8,128)(2,1)S(1)}, bf16[4,16,64]{2,1,0:T(8,128)(2,1)}, u32[]{:S(2)}) copy-start(bf16[4,16,64]{2,1,0:T(8,128)(2,1)} %param.30) | copy-start | bytes 24580
  2.6 2.3 %copy-start.8 = (bf16[4,16,64]{2,1,0:T(8,128)(2,1)S(1)}, bf16[4,16,64]{2,1,0:T(8,128)(2,1)}, u32[]{:S(2)}) copy-start(bf16[4,16,64]{2,1,0:T(8,128)(2,1)} %param.31) | copy-start | bytes 24580
  2.6 2.3 %copy-start.10 = (f32[4,16]{1,0:T(4,128)S(1)}, f32[4,16]{1,0:T(4,128)}, u32[]{:S(2)}) copy-start(f32[4,16]{1,0:T(4,128)} %param.32) | copy-start | bytes 772
  4.4 9.4 %copy-start.9 = (s32[64,2]{0,1:T(2,128)S(1)}, s32[64,2]{0,1:T(2,128)}, u32[]{:S(2)}) copy-start(s32[64,2]{0,1:T(2,128)} %param.39) | copy-start | bytes 1540
  6.2 14.4 %all-to-all-start = ((bf16[16,2,2048]{2,1,0:T(2,128)(2,1)}), bf16[16,2,2048]{2,1,0:T(2,128)(2,1)S(1)}, u32[]{:S(2)}, u32[]{:S(2)}) async-start(bf16[16,2,2048]{2,1,0:T(2,128)(2,1)} %reshape.71), calls=%async_computation | async-start | bytes 262144 | tf_op jit(solution)/shard_map/all_to_all | solution.py:24
  13.8 7.4 %copy-start.1 = (bf16[64,2048]{1,0:T(8,128)(2,1)S(1)}, bf16[64,2048]{1,0:T(8,128)(2,1)}, u32[]{:S(2)}) copy-start(bf16[64,2048]{1,0:T(8,128)(2,1)} %param.37) | copy-start | bytes 786436
  13.8 7.4 %copy-start.4 = (bf16[1024,64]{0,1:T(8,128)(2,1)S(1)}, bf16[1024,64]{0,1:T(8,128)(2,1)}, u32[]{:S(2)}) copy-start(bf16[1024,64]{0,1:T(8,128)(2,1)} %param.35) | copy-start | bytes 393220
  13.8 7.4 %copy-start.14 = (f32[64]{0:T(128)S(1)}, f32[64]{0:T(128)}, u32[]{:S(2)}) copy-start(f32[64]{0:T(128)} %param.36) | copy-start | bytes 772
  22.4 11.0 %all-to-all-start.1 = ((bf16[16,64,128]{2,1,0:T(8,128)(2,1)}), bf16[16,64,128]{2,1,0:T(8,128)(2,1)S(1)}, u32[]{:S(2)}, u32[]{:S(2)}) async-start(bf16[16,64,128]{2,1,0:T(8,128)(2,1)} %bitcast.71), calls=%async_computation.1 | async-start | bytes 524288 | tf_op jit(solution)/shard_map/all_to_all | solution.py:39
  125.0 1.2 copy-start.15
  143.3 11.5 %copy-start.13 = (f32[64,2]{0,1:T(2,128)S(1)}, f32[64,2]{0,1:T(2,128)}, u32[]{:S(2)}) copy-start(f32[64,2]{0,1:T(2,128)} %param.40) | copy-start | bytes 1540
  144.1 34.4 %all-to-all-start.6 = ((bf16[128,64,3]{0,2,1:T(4,128)(2,1)}), bf16[128,64,3]{0,2,1:T(4,128)(2,1)S(1)}, u32[]{:S(2)}, u32[]{:S(2)}) async-start(bf16[128,64,3]{0,2,1:T(4,128)(2,1)} %reshape.67), calls=%async_computation.6 | async-start | bytes 131072 | tf_op jit(solution)/shard_map/all_to_all | solution.py:168
where the time goes:
time: 180 us; the launch traced here: 179 us
  blocking collectives  104 us (58%)
  waiting for transfers between devices  35.8 us (20%)
  starting transfers between devices  20.4 us (11%)
  local copies, waits for them, and re-layouts  8.47 us (5%)
  matrix products  6.63 us (4%)
  other arithmetic  2.77 us (2%)
    all_to_all x2, blocking collectives, turned_blocks(): lax.all_to_all(parts, axes[k], split_axis=k, concat_axis=k, tiled=True)  62.2 us
    all_to_all x1, waiting for transfers between devices, local(): lax.all_to_all(back_rows, EP, split_axis=1, concat_axis=1, tiled=True)  23.3 us
    all_to_all x1, blocking collectives, from_everyone(): return lax.all_to_all(copies, axis, split_axis=0, concat_axis=0, tiled=True)  14.7 us
    all_to_all x1, blocking collectives, summed_on_arrival(): parts = lax.all_to_all(split_up(shard, dim, size), axis, 0, 0, tiled=True)  14.1 us
    psum x2, blocking collectives, one_axis_at_a_time(): return functools.reduce(lax.psum, axes, shard)  13.2 us
    all_to_all x1, starting transfers between devices, local(): lax.all_to_all(back_rows, EP, split_axis=1, concat_axis=1, tiled=True)  9.26 us
    all_to_all x1, starting transfers between devices, from_everyone(): return lax.all_to_all(copies, axis, split_axis=0, concat_axis=0, tiled=True)  7.57 us
    all_to_all x1, waiting for transfers between devices, summed_on_arrival(): parts = lax.all_to_all(split_up(shard, dim, size), axis, 0, 0, tiled=True)  6.62 us
  transfers between devices with their start and end apart: 3, of which 3 were waited for; matrix products, arithmetic and copies ran while one was open for 2% of the time, Pallas kernels for 0%

commit v1 on v0

v1 whole, which is shorter than its diff:
```python
import functools

import jax
import jax.numpy as jnp
from jax import lax
from jax.experimental import pallas as pl
from jax.experimental.pallas import tpu as pltpu
from jax.sharding import PartitionSpec as P

MESH = pl.DeviceIdType.MESH
F32 = jnp.float32
BF16 = jnp.bfloat16
norm_eps = 1e-06

CHUNKS = 4
SLOTS = 3
PAD = 4


def iota(shape, dim):
    return lax.broadcasted_iota(jnp.int32, shape, dim)


def mm(a, b):
    return jnp.dot(a, b, preferred_element_type=F32)


def mm_nt(a, b):
    return lax.dot_general(a, b, (((1,), (1,)), ((), ())), preferred_element_type=F32)


def ring_order(nz):
    order = [0]
    for k in range(1, nz // 2):
        order += [k, -k]
    return order + [nz // 2]


def kernel(
    nz,
    ntp,
    tokens_h,
    w_in_h,
    state_re_h,
    state_im_h,
    glu_h,
    out_w_h,
    gate_h,
    up_h,
    down_h,
    mix_gain,
    turn_re,
    turn_im,
    coef_re,
    coef_im,
    in_re,
    in_im,
    out_re,
    out_im,
    skip,
    glu_bias,
    ffn_gain,
    route_t,
    weight_t,
    mixed_o,
    new_re_o,
    new_im_o,
    tokens_v,
    w_in_v,
    state_re_v,
    state_im_v,
    glu_v,
    out_w_v,
    gate_v,
    up_v,
    down_v,
    sel_v,
    comb_v,
    mix_src,
    mix_buf,
    mix_all,
    part_src,
    part_buf,
    resid_v,
    out_msg,
    arr,
    rows_src,
    rows_buf,
    xn_v,
    down_src,
    down_buf,
    back_src,
    back_buf,
    ld_sem,
    send_sem,
    mix_sem,
    part_sem,
    arr_sem,
    rows_sem,
    down_sem,
    back_sem,
):
    ep = lax.axis_index("ep")
    tp = lax.axis_index("tp")
    z = ep // 2
    core = ep % 2
    experts = 2 * nz
    per = experts // CHUNKS
    crows = per * SLOTS
    seqs, width = tokens_v.shape
    order = ring_order(nz)
    place = {off % nz: i for i, off in enumerate(order)}

    def zdev(off, other):
        c = core if other == 0 else 1 - core
        return lax.rem(z + (off % nz), nz) * 2 + c

    def tdev(k):
        return lax.rem(tp + k, ntp)

    t_order = sorted(range(1, ntp), key=lambda k: -((k % 4 != 0) + (k // 4 != 0)))

    bar = pltpu.get_barrier_semaphore()
    for off in reversed(order):
        for other in (0, 1):
            if off == 0 and other == 0:
                continue
            pl.semaphore_signal(
                bar, inc=1, device_id=(zdev(off, other), tp), device_id_type=MESH
            )
    for k in range(1, ntp):
        pl.semaphore_signal(bar, inc=1, device_id=(ep, tdev(k)), device_id_type=MESH)

    loads = [
        pltpu.make_async_copy(src, dst, ld_sem.at[i])
        for i, (src, dst) in enumerate(
            [
                (tokens_h, tokens_v),
                (w_in_h, w_in_v),
                (state_re_h, state_re_v),
                (state_im_h, state_im_v),
                (glu_h, glu_v),
                (out_w_h, out_w_v),
                (gate_h.at[0], gate_v),
                (up_h.at[0], up_v),
                (down_h.at[0], down_v),
            ]
        )
    ]
    for copy in loads:
        copy.start()

    lines = experts * PAD
    expert_of = iota((lines, seqs), 0) // PAD
    slot_of = (iota((lines, seqs), 0) % PAD).astype(F32)
    before = (iota((seqs, seqs), 0) < iota((seqs, seqs), 1)).astype(BF16)
    taken = jnp.zeros((lines, 1), F32)
    sel = jnp.zeros((lines, seqs), F32)
    comb = jnp.zeros((lines, seqs), F32)
    for k in range(route_t.shape[0]):
        hits = (route_t[k : k + 1, :] == expert_of).astype(F32)
        rank = mm(hits.astype(BF16), before) + taken
        mine = jnp.where(rank == slot_of, hits, 0.0)
        taken = taken + jnp.sum(hits, axis=1, keepdims=True)
        sel = sel + mine
        comb = comb + mine * weight_t[k : k + 1, :]
    sel_v[...] = sel.astype(BF16)
    comb_hi = comb.astype(BF16)
    comb_lo = (comb - comb_hi.astype(F32)).astype(BF16)
    same = (iota((seqs, seqs), 0) == iota((seqs, seqs), 1)).astype(BF16)
    comb_v[0] = mm_nt(same, comb_hi).astype(BF16)
    comb_v[1] = mm_nt(same, comb_lo).astype(BF16)

    loads[0].wait()
    values = tokens_v[...].astype(F32)
    scale = lax.rsqrt(jnp.mean(values * values, axis=-1, keepdims=True) + norm_eps)
    normed = (values * scale * mix_gain[...]).astype(BF16)
    loads[1].wait()
    drive = mm(normed, w_in_v[...]).astype(BF16)
    loads[2].wait()
    loads[3].wait()
    chans = drive.shape[1]
    groups = turn_re.shape[0]
    chan_group = iota((chans, in_re.shape[1]), 0) // (chans // groups)
    read = skip[...] * drive.astype(F32)
    for g in range(groups):
        own = chan_group == g
        zero = jnp.zeros(own.shape, BF16)
        drive_re = mm(drive, jnp.where(own, in_re[...], zero))
        drive_im = mm(drive, jnp.where(own, in_im[...], zero))
        tr, ti = turn_re[g : g + 1, :], turn_im[g : g + 1, :]
        cr, ci = coef_re[g : g + 1, :], coef_im[g : g + 1, :]
        sr, si = state_re_v[:, g, :], state_im_v[:, g, :]
        nr = tr * sr - ti * si + (cr * drive_re - ci * drive_im)
        ni = tr * si + ti * sr + (cr * drive_im + ci * drive_re)
        new_re_o[:, g, :] = nr
        new_im_o[:, g, :] = ni
        o_re = jnp.where(own, out_re[...], zero)
        o_im = jnp.where(own, out_im[...], zero)
        for val, o_mat, sign in ((nr, o_re, 1.0), (ni, o_im, -1.0)):
            hi = val.astype(BF16)
            lo = (val - hi.astype(F32)).astype(BF16)
            read = read + sign * (mm_nt(hi, o_mat) + mm_nt(lo, o_mat))
    mixed_in = jax.nn.gelu(read).astype(BF16)

    half = seqs // 2
    row, col = iota((chans, 2 * chans), 0), iota((chans, 2 * chans), 1)
    left = (row == col).astype(BF16)
    right = (row + chans == col).astype(BF16)
    packed = mm(mixed_in[:half], left) + mm(mixed_in[half:], right)
    mix_src[...] = packed.astype(BF16)
    mix_buf[tp] = packed.astype(BF16)

    pl.semaphore_wait(bar, 2 * nz - 1 + ntp - 1)

    def to_group(src_of, dst, send, recv):
        for k in t_order:
            t = tdev(k)
            pltpu.make_async_remote_copy(
                src_ref=src_of(t),
                dst_ref=dst,
                send_sem=send,
                recv_sem=recv,
                device_id=(ep, t),
                device_id_type=MESH,
            ).start()

    def arrived(ref, sem):
        pltpu.make_async_copy(ref, ref, sem).wait()

    to_group(lambda t: mix_src, mix_buf.at[tp], send_sem.at[0], mix_sem)
    loads[4].wait()
    loads[5].wait()
    arrived(mix_buf.at[pl.ds(0, ntp - 1)], mix_sem)
    lane = iota((half, 2 * chans), 1)
    gate = jnp.zeros((seqs, chans), F32)
    for t in range(ntp):
        block = mix_buf[t]
        zero = jnp.zeros(block.shape, BF16)
        mix_all[0:half] = jnp.where(lane < chans, block, zero)
        mix_all[half:seqs] = jnp.where(lane < chans, zero, block)
        w = glu_v[t * chans : (t + 1) * chans, :]
        gate = gate + mm(mix_all[...], jnp.concatenate([w, w], axis=0))
    gated = (mixed_in.astype(F32) * jax.nn.sigmoid(gate + glu_bias[...])).astype(BF16)
    local = width // ntp
    for t in range(ntp):
        part = mm(gated, out_w_v[:, t * local : (t + 1) * local])
        part_src[t] = part.astype(BF16)
    part_buf[tp] = part_src[tp]
    to_group(lambda t: part_src.at[t], part_buf.at[tp], send_sem.at[1], part_sem)
    arrived(part_buf.at[pl.ds(0, ntp - 1)], part_sem)
    total = tokens_v[:, pl.ds(pl.multiple_of(tp * local, local), local)].astype(F32)
    mix_total = part_buf[0].astype(F32)
    for t in range(1, ntp):
        mix_total = mix_total + part_buf[t].astype(F32)
    resid = (total + mix_total).astype(BF16)
    resid_v[...] = resid

    out_msg[...] = mm(sel_v[...], resid).astype(BF16).reshape(experts, PAD, local)
    for off in reversed(order):
        for other in (0, 1):
            if off == 0 and other == 0:
                continue
            dst = zdev(off, other)
            pos = 2 * place[-off % nz] + other
            pltpu.make_async_remote_copy(
                src_ref=out_msg.at[dst],
                dst_ref=arr.at[pos],
                send_sem=send_sem.at[2],
                recv_sem=arr_sem.at[pos // per],
                device_id=(dst, tp),
                device_id_type=MESH,
            ).start()
    arr[0] = out_msg[ep]

    line, spot = iota((crows, per * PAD), 0), iota((crows, per * PAD), 1)
    compact = ((line % per) * PAD + line // per == spot).astype(BF16)
    spot2, line2 = iota((per * PAD, crows), 0), iota((per * PAD, crows), 1)
    spread = ((line2 % per) * PAD + line2 // per == spot2).astype(BF16)

    def gather(c):
        first = 1 if c == 0 else 0
        arrived(arr.at[pl.ds(c * per + first, per - first)], arr_sem.at[c])
        block = arr[c * per : (c + 1) * per].reshape(per * PAD, local)
        rows = mm(compact, block).astype(BF16)
        rows_src[c] = rows
        rows_buf[c, tp] = rows
        to_group(lambda t: rows_src.at[c], rows_buf.at[c, tp], send_sem.at[3 + c], rows_sem.at[c])

    def expert(c):
        arrived(rows_buf.at[c, pl.ds(0, ntp - 1)], rows_sem.at[c])
        squares = jnp.zeros((crows, local), F32)
        for t in range(ntp):
            v = rows_buf[c, t].astype(F32)
            squares = squares + v * v
        norm = lax.rsqrt(jnp.sum(squares, axis=1, keepdims=True) / width + norm_eps)
        for t in range(ntp):
            v = rows_buf[c, t].astype(F32)
            gain = ffn_gain[:, t * local : (t + 1) * local]
            xn_v[:, t * local : (t + 1) * local] = (v * norm * gain).astype(BF16)
        if c == 0:
            for i in (6, 7, 8):
                loads[i].wait()
        rows = xn_v[...]
        hidden = (jax.nn.silu(mm(rows, gate_v[...])) * mm(rows, up_v[...])).astype(BF16)
        for t in range(ntp):
            down_src[c, t] = mm(hidden, down_v[:, t * local : (t + 1) * local]).astype(BF16)
        down_buf[c, tp] = down_src[c, tp]
        to_group(
            lambda t: down_src.at[c, t],
            down_buf.at[c, tp],
            send_sem.at[3 + CHUNKS + c],
            down_sem.at[c],
        )

    def give_back(c):
        arrived(down_buf.at[c, pl.ds(0, ntp - 1)], down_sem.at[c])
        rows = down_buf[c, 0].astype(F32)
        for t in range(1, ntp):
            rows = rows + down_buf[c, t].astype(F32)
        rows = mm(spread, rows.astype(BF16)).astype(BF16)
        back_src[c * per : (c + 1) * per] = rows.reshape(per, PAD, local)
        for pos in reversed(range(c * per, (c + 1) * per)):
            if pos == 0:
                back_buf[ep] = back_src[0]
                continue
            dst = zdev(order[pos // 2], pos % 2)
            pltpu.make_async_remote_copy(
                src_ref=back_src.at[pos],
                dst_ref=back_buf.at[ep],
                send_sem=send_sem.at[3 + 2 * CHUNKS],
                recv_sem=back_sem,
                device_id=(dst, tp),
                device_id_type=MESH,
            ).start()

    gather(0)
    gather(1)
    expert(0)
    gather(2)
    expert(1)
    gather(3)
    expert(2)
    give_back(0)
    expert(3)
    give_back(1)
    give_back(2)
    give_back(3)

    arrived(back_buf.at[pl.ds(0, experts - 1)], back_sem)
    back = back_buf[...].reshape(lines, local)
    summed = mm(comb_v[0], back) + mm(comb_v[1], back)
    mixed_o[...] = (resid_v[...].astype(F32) + summed).astype(BF16)

    others = ntp - 1
    arrived(mix_buf.at[pl.ds(0, others)], send_sem.at[0])
    arrived(part_buf.at[pl.ds(0, others)], send_sem.at[1])
    arrived(arr.at[pl.ds(0, experts - 1)], send_sem.at[2])
    for c in range(CHUNKS):
        arrived(rows_buf.at[c, pl.ds(0, others)], send_sem.at[3 + c])
        arrived(down_buf.at[c, pl.ds(0, others)], send_sem.at[3 + CHUNKS + c])
    arrived(back_buf.at[pl.ds(0, experts - 1)], send_sem.at[3 + 2 * CHUNKS])


def local(
    nz,
    ntp,
    tokens,
    mix_gain,
    w_in,
    decay_re,
    freq,
    log_step,
    in_re,
    in_im,
    out_re,
    out_im,
    skip,
    state_re,
    state_im,
    glu_weight,
    glu_bias,
    out_weight,
    ffn_gain,
    route,
    route_weight,
    expert_gate,
    expert_up,
    expert_down,
):
    step = jnp.exp(log_step)[:, None]
    magnitude = jnp.exp(decay_re * step)
    turn_re = magnitude * jnp.cos(freq * step)
    turn_im = magnitude * jnp.sin(freq * step)
    denom = decay_re * decay_re + freq * freq
    coef_re = ((turn_re - 1.0) * decay_re + turn_im * freq) / denom
    coef_im = (turn_im * decay_re - (turn_re - 1.0) * freq) / denom

    seqs, width = tokens.shape
    chans = w_in.shape[1]
    states = decay_re.shape[1]
    loc = width // ntp
    experts = 2 * nz
    per = experts // CHUNKS
    crows = per * SLOTS
    flat = lambda m: m.reshape(chans, states)
    row = lambda v: v.reshape(1, -1)

    def vmem(*shape, dtype=BF16):
        return pltpu.VMEM(shape, dtype)

    dma = pltpu.SemaphoreType.DMA
    any_spec = pl.BlockSpec(memory_space=pl.ANY)
    vmem_spec = pl.BlockSpec(memory_space=pltpu.VMEM)
    return pl.pallas_call(
        functools.partial(kernel, nz, ntp),
        out_shape=(
            jax.ShapeDtypeStruct((seqs, loc), BF16),
            jax.ShapeDtypeStruct(state_re.shape, F32),
            jax.ShapeDtypeStruct(state_im.shape, F32),
        ),
        in_specs=[any_spec] * 9 + [vmem_spec] * 14,
        out_specs=(vmem_spec,) * 3,
        scratch_shapes=[
            vmem(*tokens.shape),
            vmem(*w_in.shape),
            vmem(*state_re.shape, dtype=F32),
            vmem(*state_im.shape, dtype=F32),
            vmem(*glu_weight.shape),
            vmem(*out_weight.shape),
            vmem(*expert_gate.shape[1:]),
            vmem(*expert_up.shape[1:]),
            vmem(*expert_down.shape[1:]),
            vmem(experts * PAD, seqs),
            vmem(2, seqs, experts * PAD),
            vmem(seqs // 2, 2 * chans),
            vmem(ntp, seqs // 2, 2 * chans),
            vmem(seqs, 2 * chans),
            vmem(ntp, seqs, loc),
            vmem(ntp, seqs, loc),
            vmem(seqs, loc),
            vmem(experts, PAD, loc),
            vmem(experts, PAD, loc),
            vmem(CHUNKS, crows, loc),
            vmem(CHUNKS, ntp, crows, loc),
            vmem(crows, width),
            vmem(CHUNKS, ntp, crows, loc),
            vmem(CHUNKS, ntp, crows, loc),
            vmem(experts, PAD, loc),
            vmem(experts, PAD, loc),
            dma((9,)),
            dma((4 + 2 * CHUNKS,)),
            dma,
            dma,
            dma((CHUNKS,)),
            dma((CHUNKS,)),
            dma((CHUNKS,)),
            dma,
        ],
        compiler_params=pltpu.CompilerParams(collective_id=0, has_side_effects=True),
    )(
        tokens,
        w_in,
        state_re,
        state_im,
        glu_weight,
        out_weight,
        expert_gate,
        expert_up,
        expert_down,
        row(mix_gain),
        turn_re,
        turn_im,
        coef_re,
        coef_im,
        flat(in_re),
        flat(in_im),
        flat(out_re),
        flat(out_im),
        row(skip),
        row(glu_bias),
        row(ffn_gain),
        route.T,
        route_weight.T,
    )


def solution(mesh):
    ep, tp = mesh.axis_names
    placed = (
        P(ep, None),
        P(),
        P(None, tp),
        P(tp, None),
        P(tp, None),
        P(tp),
        P(tp, None, None),
        P(tp, None, None),
        P(tp, None, None),
        P(tp, None, None),
        P(tp, None),
        P(ep, tp, None),
        P(ep, tp, None),
        P(None, tp),
        P(tp),
        P(tp, None),
        P(),
        P(ep, None),
        P(ep, None),
        P(ep, None, tp),
        P(ep, None, tp),
        P(ep, tp, None),
    )
    return jax.shard_map(
        functools.partial(local, mesh.shape[ep] // 2, mesh.shape[tp]),
        mesh=mesh,
        in_specs=placed,
        out_specs=(P(ep, tp), P(ep, tp, None), P(ep, tp, None)),
        check_vma=False,
    )
```

time: 180 us -> 101 us (0.56)
  blocking collectives: 104 us -> 0 us
  Pallas kernels: 0 us -> 86.7 us
  waiting for transfers between devices: 35.8 us -> 0 us
  starting transfers between devices: 20.4 us -> 0 us
  matrix products: 6.63 us -> 0 us
  local copies, waits for them, and re-layouts: 8.47 us -> 11.9 us
    all_to_all x4 -> x0, blocking collectives: 91 us -> none  [the longest x2 62.2 us: turned_blocks(): lax.all_to_all(parts, axes[k], split_axis=k, concat_axis=k, tiled=True)]
    pallas_call x0 -> x1, Pallas kernels: none -> 86.7 us  [local(): pl.pallas_call(functools.partial(kernel, nz, ntp), out_shape=(jax.ShapeDt...]
    all_to_all x3 -> x0, waiting for transfers between devices: 35.8 us -> none  [the longest x1 23.3 us: local(): lax.all_to_all(back_rows, EP, split_axis=1, concat_axis=1, tiled=True)]
    all_to_all x3 -> x0, starting transfers between devices: 20.4 us -> none  [the longest x1 9.26 us: local(): lax.all_to_all(back_rows, EP, split_axis=1, concat_axis=1, tiled=True)]
    psum x2 -> x0, blocking collectives: 13.2 us -> none  [one_axis_at_a_time(): return functools.reduce(lax.psum, axes, shard)]
    dot_general x11 -> x0, matrix products: 6.63 us -> none  [the longest x1 2.31 us: local(): lax.dot_general(down_local, hidden, (((0,), (1,)), ((), ())), preferred_e...]
    unnamed x38 -> x13, local copies, waits for them, and re-layouts: 3.54 us -> 9.87 us
    reduce_sum x5 -> x0, other arithmetic: 2.28 us -> none  [the longest x1 1.12 us: rms_scale(): jnp.mean(values * values, axis=-1, keepdims=True) + norm_eps]
  transfers between devices with their start and end apart: 3 -> 0, of which waited for: 3 -> 0; matrix products, arithmetic and copies ran while one was open for 2% -> 0% of each run, Pallas kernels for 0% -> 0%
where the time goes in v1:
time: 101 us
  Pallas kernels  86.7 us (86%)
  local copies, waits for them, and re-layouts  11.9 us (12%)
  other arithmetic  1.41 us (1%)
    pallas_call x1, Pallas kernels, local(): pl.pallas_call(functools.partial(kernel, nz, ntp), out_shape=(jax.ShapeDt...  86.7 us
    unnamed x13, local copies, waits for them, and re-layouts  9.87 us

profile of v1, /device:TPU:1, one launch (start us, length us, event | category | flops | bytes accessed | tf_op | source)
XLA Modules:
  0.0 100.6 jit_solution(1395916358111879985)
XLA Ops:
  0.6 0.0 copy-start
  0.6 0.7 exp.6
  1.4 1.3 %reshape.36.skip = f32[1,64]{1,0:T(1,128)} reshape(f32[4,16]{1,0:T(4,128)} %param.32) | data formatting | bytes 512 | tf_op jit(solution)/shard_map/reshape | solution.py:407
  2.7 1.4 %subtract_divide_fusion = (f32[4,64]{1,0:T(4,128)}, f32[4,64]{1,0:T(4,128)}, f32[4,64]{1,0:T(4,128)}, f32[4,64]{1,0:T(4,128)}) fusion(f32[4,64]{1,0:T(4,128)} %param.26, f32[4,64]{1,0:T(4,128)} %param.25, f32[4]{0:T(128)S(1)} %exp.6), kind=kLoop, calls=%fused_computation | loop fusion | flops 4096 | bytes 6160 | tf_op jit(solution)/shard_map/div | solution.py:397
  4.1 1.7 %copy.26.glu_h = bf16[1024,64]{1,0:T(8,128)(2,1)} copy(bf16[1024,64]{0,1:T(8,128)(2,1)} %param.35) | data formatting | bytes 262144 | tf_op args[13]
  5.8 2.0 %copy.25.w_in_h = bf16[2048,64]{1,0:T(8,128)(2,1)} copy(bf16[2048,64]{0,1:T(8,128)(2,1)} %param.24) | data formatting | bytes 524288 | tf_op args[2]
  7.8 0.0 copy-done
  7.8 0.0 copy-start.1
  7.8 1.3 %copy.27.gate_h = bf16[1,2048,224]{2,1,0:T(8,128)(2,1)} copy(bf16[1,2048,224]{1,2,0:T(8,128)(2,1)S(1)} %copy-done) | data formatting | bytes 1835008 | tf_op args[19]
  9.1 0.0 copy-done.1
  9.1 1.3 %copy.28.up_h = bf16[1,2048,224]{2,1,0:T(8,128)(2,1)} copy(bf16[1,2048,224]{1,2,0:T(8,128)(2,1)S(1)} %copy-done.1) | data formatting | bytes 1835008 | tf_op args[20]
  10.4 86.7 %shard_map.229 = (bf16[64,128]{1,0:T(8,128)(2,1)}, f32[64,4,64]{2,1,0:T(4,128)}, f32[64,4,64]{2,1,0:T(4,128)}) custom-call(bf16[64,2048]{1,0:T(8,128)(2,1)} %tokens_h.1, bf16[2048,64]{1,0:T(8,128)(2,1)} %copy.25.w_in_h, f32[64,4,64]{2,1,0:T(4,128)} %state_re_h.1, f32[64,4,64]{2,1,0:T(4,128)} %state_im_h.1, bf16[1024,64]{1,0:T(8,128)(2,1)} %copy.26.glu_h, ...), custom_call_target="tpu_custom_call" | custom-call | tf_op jit(solution)/shard_map/pallas_call | solution.py:415
  97.1 1.3 %copy.32 = bf16[64,128]{1,0:T(8,128)(2,1)} copy(bf16[64,128]{1,0:T(8,128)(2,1)} %get-tuple-element.10) | data formatting | bytes 32768
  98.4 0.0 copy-start.2
  98.4 1.6 %copy.33 = f32[64,4,64]{2,1,0:T(4,128)} copy(f32[64,4,64]{2,1,0:T(4,128)} %get-tuple-element.11) | data formatting | bytes 131072
  100.0 0.0 copy-done.2
  100.0 0.7 copy.34
Async XLA Ops:
  0.6 7.1 %copy-start = (bf16[1,2048,224]{1,2,0:T(8,128)(2,1)S(1)}, bf16[1,2048,224]{1,2,0:T(8,128)(2,1)}, u32[]{:S(2)}) copy-start(bf16[1,2048,224]{1,2,0:T(8,128)(2,1)} %param.41) | copy-start | bytes 2752516
  7.8 1.3 %copy-start.1 = (bf16[1,2048,224]{1,2,0:T(8,128)(2,1)S(1)}, bf16[1,2048,224]{1,2,0:T(8,128)(2,1)}, u32[]{:S(2)}) copy-start(bf16[1,2048,224]{1,2,0:T(8,128)(2,1)} %param.42) | copy-start | bytes 2752516
  98.4 1.6 %copy-start.2 = (f32[64,4,64]{2,1,0:T(4,128)S(1)}, f32[64,4,64]{2,1,0:T(4,128)}, u32[]{:S(2)}) copy-start(f32[64,4,64]{2,1,0:T(4,128)} %get-tuple-element.12) | copy-start | bytes 196612

commit v2 on v1

v2 whole, which is shorter than its diff:
```python
import functools

import jax
import jax.numpy as jnp
from jax import lax
from jax.experimental import pallas as pl
from jax.experimental.pallas import tpu as pltpu
from jax.sharding import PartitionSpec as P

MESH = pl.DeviceIdType.MESH
F32 = jnp.float32
BF16 = jnp.bfloat16
norm_eps = 1e-06

CHUNKS = 4
SLOTS = 3
PAD = 4


def iota(shape, dim):
    return lax.broadcasted_iota(jnp.int32, shape, dim)


def mm(a, b):
    return jnp.dot(a, b, preferred_element_type=F32)


def mm_nt(a, b):
    return lax.dot_general(a, b, (((1,), (1,)), ((), ())), preferred_element_type=F32)


def ring_order(nz):
    order = [0]
    for k in range(1, nz // 2):
        order += [k, -k]
    return order + [nz // 2]


INPUTS = (
    "route_t",
    "weight_t",
    "log_step",
    "decay_re",
    "freq",
    "skip",
    "in_re",
    "in_im",
    "out_re",
    "out_im",
    "mix_gain",
    "tokens",
    "w_in_t",
    "state_re",
    "state_im",
    "glu_bias",
    "glu_t",
    "out_w",
    "ffn_gain",
    "gate_t",
    "up_t",
    "down",
)


def kernel(nz, ntp, *refs):
    hbm = dict(zip(INPUTS, refs))
    refs = refs[len(INPUTS) :]
    mixed_o, new_re_o, new_im_o = refs[:3]
    v = dict(zip(INPUTS, refs[3:]))
    (
        sel_v,
        comb_v,
        glu_s,
        mix_src,
        mix_buf,
        mix_all,
        part_src,
        part_buf,
        resid_v,
        out_msg,
        arr,
        rows_src,
        rows_buf,
        xn_v,
        down_src,
        down_buf,
        back_src,
        back_buf,
        ld_sem,
        send_sem,
        mix_sem,
        part_sem,
        arr_sem,
        rows_sem,
        down_sem,
        back_sem,
        near_sem,
    ) = refs[3 + len(INPUTS) :]
    ep = lax.axis_index("ep")
    tp = lax.axis_index("tp")
    z = ep // 2
    core = ep % 2
    experts = 2 * nz
    per = experts // CHUNKS
    crows = per * SLOTS
    seqs, width = v["tokens"].shape
    order = ring_order(nz)

    def zdev(off, other):
        c = core if other == 0 else 1 - core
        return lax.rem(z + (off % nz), nz) * 2 + c

    def tdev(k):
        return lax.rem(tp + k, ntp)

    def signal(sem, dst):
        pl.semaphore_signal(sem, inc=1, device_id=dst, device_id_type=MESH)

    reach = nz // 8
    near = [(off, o) for off in order if abs(off) <= reach for o in (0, 1)]
    near.remove((0, 0))
    bar = pltpu.get_barrier_semaphore()
    for off, other in reversed(near):
        signal(bar, (zdev(off, other), tp))
    for k in range(1, ntp):
        signal(bar, (ep, tdev(k)))

    loads = {
        n: pltpu.make_async_copy(hbm[n], v[n], ld_sem.at[i]) for i, n in enumerate(INPUTS)
    }
    for n in INPUTS:
        loads[n].start()

    def loaded(*names):
        for n in names:
            loads[n].wait()

    loaded("log_step", "decay_re", "freq")
    decay_re, freq = v["decay_re"][...], v["freq"][...]
    groups, states = decay_re.shape
    group = iota((groups, states), 0)
    log_step = jnp.zeros((groups, states), F32)
    for g in range(groups):
        log_step = jnp.where(group == g, v["log_step"][0:1, g : g + 1], log_step)
    step = jnp.exp(log_step)
    magnitude = jnp.exp(decay_re * step)
    turn_re = magnitude * jnp.cos(freq * step)
    turn_im = magnitude * jnp.sin(freq * step)
    denom = decay_re * decay_re + freq * freq
    coef_re = ((turn_re - 1.0) * decay_re + turn_im * freq) / denom
    coef_im = (turn_im * decay_re - (turn_re - 1.0) * freq) / denom

    loaded("skip", "in_re", "in_im", "out_re", "out_im", "mix_gain", "tokens")
    values = v["tokens"][...].astype(F32)
    scale = lax.rsqrt(jnp.mean(values * values, axis=-1, keepdims=True) + norm_eps)
    normed = (values * scale * v["mix_gain"][...]).astype(BF16)
    loaded("w_in_t")
    drive = mm_nt(normed, v["w_in_t"][...]).astype(BF16)
    chans = drive.shape[1]
    places = chans // groups
    chan_group = iota((chans, states), 0) // places
    spread_h = (iota((places, chans), 0) == iota((places, chans), 1) % places).astype(BF16)
    skip_rows = jnp.zeros((groups, chans), F32)
    rest = v["skip"][...]
    for _ in range(3):
        piece = rest.astype(BF16)
        skip_rows = skip_rows + mm(piece, spread_h)
        rest = rest - piece.astype(F32)
    of_group = iota((groups, chans), 0) == iota((groups, chans), 1) // places
    skip = jnp.sum(jnp.where(of_group, skip_rows, 0.0), axis=0, keepdims=True)
    read = skip * drive.astype(F32)
    loaded("state_re", "state_im")
    for g in range(groups):
        own = chan_group == g
        zero = jnp.zeros(own.shape, BF16)
        drive_re = mm(drive, jnp.where(own, v["in_re"][...], zero))
        drive_im = mm(drive, jnp.where(own, v["in_im"][...], zero))
        tr, ti = turn_re[g : g + 1, :], turn_im[g : g + 1, :]
        cr, ci = coef_re[g : g + 1, :], coef_im[g : g + 1, :]
        sr, si = v["state_re"][:, g, :], v["state_im"][:, g, :]
        nr = tr * sr - ti * si + (cr * drive_re - ci * drive_im)
        ni = tr * si + ti * sr + (cr * drive_im + ci * drive_re)
        new_re_o[:, g, :] = nr
        new_im_o[:, g, :] = ni
        o_re = jnp.where(own, v["out_re"][...], zero)
        o_im = jnp.where(own, v["out_im"][...], zero)
        for val, o_mat, sign in ((nr, o_re, 1.0), (ni, o_im, -1.0)):
            hi = val.astype(BF16)
            lo = (val - hi.astype(F32)).astype(BF16)
            read = read + sign * (mm_nt(hi, o_mat) + mm_nt(lo, o_mat))
    mixed_in = jax.nn.gelu(read).astype(BF16)

    half = seqs // 2
    row, col = iota((chans, 2 * chans), 0), iota((chans, 2 * chans), 1)
    left = (row == col).astype(BF16)
    right = (row + chans == col).astype(BF16)
    packed = mm(mixed_in[:half], left) + mm(mixed_in[half:], right)
    mix_src[...] = packed.astype(BF16)
    mix_buf[tp] = packed.astype(BF16)

    pl.semaphore_wait(bar, len(near) + ntp - 1)
    def pass_on(i):
        for off in (reach << i, -(reach << i)):
            signal(near_sem.at[i], (zdev(off, 0), tp))

    pass_on(0)

    t_order = sorted(range(1, ntp), key=lambda k: -((k % 4 != 0) + (k // 4 != 0)))

    def to_group(src_of, dst, send, recv):
        for k in t_order:
            t = tdev(k)
            pltpu.make_async_remote_copy(
                src_ref=src_of(t),
                dst_ref=dst,
                send_sem=send,
                recv_sem=recv,
                device_id=(ep, t),
                device_id_type=MESH,
            ).start()

    def arrived(ref, sem):
        pltpu.make_async_copy(ref, ref, sem).wait()

    to_group(lambda t: mix_src, mix_buf.at[tp], send_sem.at[0], mix_sem)

    loaded("glu_t", "glu_bias", "out_w")
    wide = 2 * chans
    same = (iota((wide, wide), 0) == iota((wide, wide), 1)).astype(BF16)
    for p in range(ntp // 2):
        w = mm_nt(same, v["glu_t"][:, p * wide : (p + 1) * wide]).astype(BF16)
        for i in (0, 1):
            t = 2 * p + i
            for j in (0, 1):
                at = t * wide + j * chans
                glu_s[at : at + chans, :] = w[i * chans : (i + 1) * chans, :]

    arrived(mix_buf.at[pl.ds(0, ntp - 1)], mix_sem)
    pl.semaphore_wait(near_sem.at[0], 2)
    pass_on(1)
    lane = iota((half, wide), 1)
    for t in range(ntp):
        block = mix_buf[t]
        zero = jnp.zeros(block.shape, BF16)
        mix_all[0:half, t * wide : (t + 1) * wide] = jnp.where(lane < chans, block, zero)
        mix_all[half:seqs, t * wide : (t + 1) * wide] = jnp.where(lane < chans, zero, block)
    gate = mm(mix_all[...], glu_s[...]) + v["glu_bias"][...]
    gated = (mixed_in.astype(F32) * jax.nn.sigmoid(gate)).astype(BF16)
    local = width // ntp
    step_t = 4
    for t0 in range(0, ntp, step_t):
        part = mm(gated, v["out_w"][:, t0 * local : (t0 + step_t) * local]).astype(BF16)
        for i in range(step_t):
            part_src[t0 + i] = part[:, i * local : (i + 1) * local]
    to_group(lambda t: part_src.at[t], part_buf.at[tp], send_sem.at[1], part_sem)
    part_buf[tp] = part_src[tp]

    loaded("route_t", "weight_t")
    lines = experts * PAD
    expert_of = iota((lines, seqs), 0) // PAD
    slot_of = (iota((lines, seqs), 0) % PAD).astype(F32)
    before = (iota((seqs, seqs), 0) < iota((seqs, seqs), 1)).astype(BF16)
    taken = jnp.zeros((lines, 1), F32)
    sel = jnp.zeros((lines, seqs), F32)
    comb = jnp.zeros((lines, seqs), F32)
    for k in range(v["route_t"].shape[0]):
        hits = (v["route_t"][k : k + 1, :] == expert_of).astype(F32)
        rank = mm(hits.astype(BF16), before) + taken
        mine = jnp.where(rank == slot_of, hits, 0.0)
        taken = taken + jnp.sum(hits, axis=1, keepdims=True)
        sel = sel + mine
        comb = comb + mine * v["weight_t"][k : k + 1, :]
    sel_v[...] = sel.astype(BF16)
    comb_hi = comb.astype(BF16)
    comb_lo = (comb - comb_hi.astype(F32)).astype(BF16)
    eye = (iota((seqs, seqs), 0) == iota((seqs, seqs), 1)).astype(BF16)
    comb_v[0] = mm_nt(eye, comb_hi).astype(BF16)
    comb_v[1] = mm_nt(eye, comb_lo).astype(BF16)

    total = v["tokens"][:, pl.ds(pl.multiple_of(tp * local, local), local)].astype(F32)
    arrived(part_buf.at[pl.ds(0, ntp - 1)], part_sem)
    mix_total = part_buf[0].astype(F32)
    for t in range(1, ntp):
        mix_total = mix_total + part_buf[t].astype(F32)
    resid = (total + mix_total).astype(BF16)
    resid_v[...] = resid

    out_msg[...] = mm(sel_v[...], resid).astype(BF16).reshape(experts, PAD, local)
    pl.semaphore_wait(near_sem.at[1], 2)
    chunk = z // (nz // CHUNKS)
    for off in reversed(order):
        for other in (0, 1):
            if off == 0 and other == 0:
                continue
            dst = zdev(off, other)
            pltpu.make_async_remote_copy(
                src_ref=out_msg.at[dst],
                dst_ref=arr.at[ep],
                send_sem=send_sem.at[2],
                recv_sem=arr_sem.at[chunk],
                device_id=(dst, tp),
                device_id_type=MESH,
            ).start()
    pltpu.make_async_copy(out_msg.at[ep], arr.at[ep], arr_sem.at[chunk]).start()

    line, spot = iota((crows, per * PAD), 0), iota((crows, per * PAD), 1)
    compact = ((line % per) * PAD + line // per == spot).astype(BF16)
    spot2, line2 = iota((per * PAD, crows), 0), iota((per * PAD, crows), 1)
    spread = ((line2 % per) * PAD + line2 // per == spot2).astype(BF16)

    def gather(c):
        arrived(arr.at[pl.ds(c * per, per)], arr_sem.at[c])
        block = arr[c * per : (c + 1) * per].reshape(per * PAD, local)
        rows = mm(compact, block).astype(BF16)
        rows_src[c] = rows
        to_group(lambda t: rows_src.at[c], rows_buf.at[c, tp], send_sem.at[3 + c], rows_sem.at[c])
        rows_buf[c, tp] = rows

    def expert(c, first=False):
        arrived(rows_buf.at[c, pl.ds(0, ntp - 1)], rows_sem.at[c])
        if first:
            loaded("ffn_gain")
        squares = jnp.zeros((crows, local), F32)
        for t in range(ntp):
            x = rows_buf[c, t].astype(F32)
            squares = squares + x * x
        norm = lax.rsqrt(jnp.sum(squares, axis=1, keepdims=True) / width + norm_eps)
        for t in range(ntp):
            x = rows_buf[c, t].astype(F32)
            gain = v["ffn_gain"][:, t * local : (t + 1) * local]
            xn_v[:, t * local : (t + 1) * local] = (x * norm * gain).astype(BF16)
        if first:
            loaded("gate_t", "up_t", "down")
        rows = xn_v[...]
        hidden = jax.nn.silu(mm_nt(rows, v["gate_t"][...])) * mm_nt(rows, v["up_t"][...])
        hidden = hidden.astype(BF16)
        for t0 in range(0, ntp, step_t):
            y = mm(hidden, v["down"][:, t0 * local : (t0 + step_t) * local]).astype(BF16)
            for i in range(step_t):
                down_src[c, t0 + i] = y[:, i * local : (i + 1) * local]
        to_group(
            lambda t: down_src.at[c, t],
            down_buf.at[c, tp],
            send_sem.at[3 + CHUNKS + c],
            down_sem.at[c],
        )
        down_buf[c, tp] = down_src[c, tp]

    def give_back(c):
        arrived(down_buf.at[c, pl.ds(0, ntp - 1)], down_sem.at[c])
        rows = down_buf[c, 0].astype(F32)
        for t in range(1, ntp):
            rows = rows + down_buf[c, t].astype(F32)
        rows = mm(spread, rows.astype(BF16)).astype(BF16)
        back_src[c * per : (c + 1) * per] = rows.reshape(per, PAD, local)
        for dst in range(c * per, (c + 1) * per):

            @pl.when(ep != dst)
            def _():
                pltpu.make_async_remote_copy(
                    src_ref=back_src.at[dst],
                    dst_ref=back_buf.at[ep],
                    send_sem=send_sem.at[3 + 2 * CHUNKS],
                    recv_sem=back_sem,
                    device_id=(dst, tp),
                    device_id_type=MESH,
                ).start()

        @pl.when(chunk == c)
        def _():
            pltpu.make_async_copy(back_src.at[ep], back_buf.at[ep], back_sem).start()

    gather(0)
    gather(1)
    gather(2)
    expert(0, True)
    expert(2)
    gather(3)
    expert(1)
    give_back(0)
    expert(3)
    give_back(1)
    give_back(2)
    give_back(3)

    arrived(back_buf, back_sem)
    back = back_buf[...].reshape(lines, local)
    summed = mm(comb_v[0], back) + mm(comb_v[1], back)
    mixed_o[...] = (resid_v[...].astype(F32) + summed).astype(BF16)

    others = ntp - 1
    arrived(mix_buf.at[pl.ds(0, others)], send_sem.at[0])
    arrived(part_buf.at[pl.ds(0, others)], send_sem.at[1])
    arrived(arr.at[pl.ds(0, experts - 1)], send_sem.at[2])
    for c in range(CHUNKS):
        arrived(rows_buf.at[c, pl.ds(0, others)], send_sem.at[3 + c])
        arrived(down_buf.at[c, pl.ds(0, others)], send_sem.at[3 + CHUNKS + c])
    arrived(back_buf.at[pl.ds(0, experts - 1)], send_sem.at[3 + 2 * CHUNKS])


def local(
    nz,
    ntp,
    tokens,
    mix_gain,
    w_in,
    decay_re,
    freq,
    log_step,
    in_re,
    in_im,
    out_re,
    out_im,
    skip,
    state_re,
    state_im,
    glu_weight,
    glu_bias,
    out_weight,
    ffn_gain,
    route,
    route_weight,
    expert_gate,
    expert_up,
    expert_down,
):
    seqs, width = tokens.shape
    chans = w_in.shape[1]
    states = decay_re.shape[1]
    loc = width // ntp
    experts = 2 * nz
    per = experts // CHUNKS
    crows = per * SLOTS
    flat = lambda m: m.reshape(chans, states)
    row = lambda x: x.reshape(1, -1)

    def vmem(*shape, dtype=BF16):
        return pltpu.VMEM(shape, dtype)

    inputs = dict(
        route_t=route.T,
        weight_t=route_weight.T,
        log_step=row(log_step),
        decay_re=decay_re,
        freq=freq,
        skip=skip,
        in_re=flat(in_re),
        in_im=flat(in_im),
        out_re=flat(out_re),
        out_im=flat(out_im),
        mix_gain=row(mix_gain),
        tokens=tokens,
        w_in_t=w_in.T,
        state_re=state_re,
        state_im=state_im,
        glu_bias=row(glu_bias),
        glu_t=glu_weight.T,
        out_w=out_weight,
        ffn_gain=row(ffn_gain),
        gate_t=expert_gate[0].T,
        up_t=expert_up[0].T,
        down=expert_down[0],
    )
    operands = [inputs[n] for n in INPUTS]
    dma = pltpu.SemaphoreType.DMA
    any_spec = pl.BlockSpec(memory_space=pl.ANY)
    vmem_spec = pl.BlockSpec(memory_space=pltpu.VMEM)
    outs = (
        jax.ShapeDtypeStruct((seqs, loc), BF16),
        jax.ShapeDtypeStruct(state_re.shape, F32),
        jax.ShapeDtypeStruct(state_im.shape, F32),
    )
    made = pl.pallas_call(
        functools.partial(kernel, nz, ntp),
        out_shape=tuple(pltpu.VMEM(o.shape, o.dtype) for o in outs),
        in_specs=[any_spec] * len(operands),
        out_specs=(vmem_spec,) * 3,
        scratch_shapes=[vmem(*x.shape, dtype=x.dtype) for x in operands]
        + [
            vmem(experts * PAD, seqs),
            vmem(2, seqs, experts * PAD),
            vmem(ntp * 2 * chans, chans),
            vmem(seqs // 2, 2 * chans),
            vmem(ntp, seqs // 2, 2 * chans),
            vmem(seqs, ntp * 2 * chans),
            vmem(ntp, seqs, loc),
            vmem(ntp, seqs, loc),
            vmem(seqs, loc),
            vmem(experts, PAD, loc),
            vmem(experts, PAD, loc),
            vmem(CHUNKS, crows, loc),
            vmem(CHUNKS, ntp, crows, loc),
            vmem(crows, width),
            vmem(CHUNKS, ntp, crows, loc),
            vmem(CHUNKS, ntp, crows, loc),
            vmem(experts, PAD, loc),
            vmem(experts, PAD, loc),
            dma((len(operands),)),
            dma((4 + 2 * CHUNKS,)),
            dma,
            dma,
            dma((CHUNKS,)),
            dma((CHUNKS,)),
            dma((CHUNKS,)),
            dma,
            pltpu.SemaphoreType.REGULAR((2,)),
        ],
        compiler_params=pltpu.CompilerParams(collective_id=0, has_side_effects=True),
    )(*operands)
    return made


def solution(mesh):
    ep, tp = mesh.axis_names
    placed = (
        P(ep, None),
        P(),
        P(None, tp),
        P(tp, None),
        P(tp, None),
        P(tp),
        P(tp, None, None),
        P(tp, None, None),
        P(tp, None, None),
        P(tp, None, None),
        P(tp, None),
        P(ep, tp, None),
        P(ep, tp, None),
        P(None, tp),
        P(tp),
        P(tp, None),
        P(),
        P(ep, None),
        P(ep, None),
        P(ep, None, tp),
        P(ep, None, tp),
        P(ep, tp, None),
    )
    return jax.shard_map(
        functools.partial(local, mesh.shape[ep] // 2, mesh.shape[tp]),
        mesh=mesh,
        in_specs=placed,
        out_specs=(P(ep, tp), P(ep, tp, None), P(ep, tp, None)),
        check_vma=False,
    )
```

time: 101 us -> 74.2 us (0.73)
  Pallas kernels: 86.7 us -> 71.5 us
  local copies, waits for them, and re-layouts: 11.9 us -> 1.92 us
  other arithmetic: 1.41 us -> 0 us
    pallas_call x1, Pallas kernels: 86.7 us -> 71.5 us  [local(): pl.pallas_call(functools.partial(kernel, nz, ntp), out_shape=tuple((pltpu...]
    unnamed x13 -> x3, local copies, waits for them, and re-layouts: 9.87 us -> 1.92 us
    div x1 -> x0, other arithmetic: 1.41 us -> none  [local(): coef_im = (turn_im * decay_re - (turn_re - 1.0) * freq) / denom]
    reshape x1 -> x0, local copies, waits for them, and re-layouts: 1.28 us -> none  [local(): row = lambda v: v.reshape(1, -1)]
where the time goes in v2:
time: 74.2 us; the launch traced here: 74 us
  Pallas kernels  71.5 us (96%)
  local copies, waits for them, and re-layouts  1.92 us (3%)
    pallas_call x1, Pallas kernels, local(): pl.pallas_call(functools.partial(kernel, nz, ntp), out_shape=tuple((pltpu...  71.5 us
    unnamed x3, local copies, waits for them, and re-layouts  1.92 us

profile of v2, /device:TPU:1, one launch (start us, length us, event | category | flops | bytes accessed | tf_op | source)
XLA Modules:
  0.0 74.0 jit_solution(978742005959652862)
XLA Ops:
  0.6 71.5 %shard_map.229 = (bf16[64,128]{1,0:T(8,128)(2,1)S(1)}, f32[64,4,64]{2,1,0:T(4,128)S(1)}, f32[64,4,64]{2,1,0:T(4,128)S(1)}) custom-call(s32[2,64]{1,0:T(2,128)} %bitcast.30, f32[2,64]{1,0:T(2,128)} %bitcast.31, f32[1,4]{1,0:T(1,128)} %bitcast.32, f32[4,64]{1,0:T(4,128)} %refs_3_.1, f32[4,64]{1,0:T(4,128)} %refs_4_.1, f32[4,16]{1,0:T(4,128)} %refs_5_.1, ...), custom_call_target="tpu_custom_call" | custom-call | tf_op jit(solution)/shard_map/pallas_call | solution.py:473
  72.1 0.6 copy.28
  72.7 0.7 copy.29
  73.4 0.7 copy.30

commit v3 on v2

--- a/solution.py
+++ b/solution.py
@@ -27,13 +27,6 @@
 
 def mm_nt(a, b):
     return lax.dot_general(a, b, (((1,), (1,)), ((), ())), preferred_element_type=F32)
-
-
-def ring_order(nz):
-    order = [0]
-    for k in range(1, nz // 2):
-        order += [k, -k]
-    return order + [nz // 2]
 
 
 INPUTS = (
@@ -95,6 +88,9 @@
         down_sem,
         back_sem,
         near_sem,
+        hand,
+        hand_sem,
+        wrap_sem,
     ) = refs[3 + len(INPUTS) :]
     ep = lax.axis_index("ep")
     tp = lax.axis_index("tp")
@@ -104,7 +100,6 @@
     per = experts // CHUNKS
     crows = per * SLOTS
     seqs, width = v["tokens"].shape
-    order = ring_order(nz)
 
     def zdev(off, other):
         c = core if other == 0 else 1 - core
@@ -116,12 +111,21 @@
     def signal(sem, dst):
         pl.semaphore_signal(sem, inc=1, device_id=dst, device_id_type=MESH)
 
-    reach = nz // 8
-    near = [(off, o) for off in order if abs(off) <= reach for o in (0, 1)]
-    near.remove((0, 0))
+    reach = nz // 4
+    has_prev = 1 - (nz - z) // nz
+    has_next = 1 - (z + 1) // nz
+    is_last = (z + reach) // nz
     bar = pltpu.get_barrier_semaphore()
-    for off, other in reversed(near):
-        signal(bar, (zdev(off, other), tp))
+
+    def both(off):
+        for other in (0, 1):
+            signal(bar, (zdev(off, other), tp))
+
+    for d in range(reach, 0, -1):
+        pl.when(z < d)(functools.partial(both, -d))
+    pl.when(z > 0)(functools.partial(both, -1))
+    pl.when(z < nz - 1)(functools.partial(both, 1))
+    signal(bar, (zdev(0, 1), tp))
     for k in range(1, ntp):
         signal(bar, (ep, tdev(k)))
 
@@ -198,12 +202,32 @@
     mix_src[...] = packed.astype(BF16)
     mix_buf[tp] = packed.astype(BF16)
 
-    pl.semaphore_wait(bar, len(near) + ntp - 1)
+    firsts = 2 * is_last * (z - (nz - reach) + 1)
+    pl.semaphore_wait(bar, ntp + 2 * has_prev + 2 * has_next + firsts)
+
+    rounds = (1, 2, 4)
+
     def pass_on(i):
-        for off in (reach << i, -(reach << i)):
-            signal(near_sem.at[i], (zdev(off, 0), tp))
+        r = rounds[i]
+
+        @pl.when(z >= r)
+        def _():
+            signal(near_sem.at[i], (zdev(-r, 0), tp))
+
+        @pl.when(z < nz - r)
+        def _():
+            signal(near_sem.at[i], (zdev(r, 0), tp))
+
+    def heard(i):
+        r = rounds[i]
+        pl.semaphore_wait(near_sem.at[i], 2 - (nz - 1 - z + r) // nz - (z + r) // nz)
 
     pass_on(0)
+    for d in range(reach, 0, -1):
+
+        @pl.when(z >= nz - d)
+        def _():
+            signal(wrap_sem, (zdev(d, 0), tp))
 
     t_order = sorted(range(1, ntp), key=lambda k: -((k % 4 != 0) + (k // 4 != 0)))
 
@@ -235,9 +259,11 @@
                 at = t * wide + j * chans
                 glu_s[at : at + chans, :] = w[i * chans : (i + 1) * chans, :]
 
+    heard(0)
+    pass_on(1)
+    heard(1)
+    pass_on(2)
     arrived(mix_buf.at[pl.ds(0, ntp - 1)], mix_sem)
-    pl.semaphore_wait(near_sem.at[0], 2)
-    pass_on(1)
     lane = iota((half, wide), 1)
     for t in range(ntp):
         block = mix_buf[t]
@@ -286,22 +312,63 @@
     resid_v[...] = resid
 
     out_msg[...] = mm(sel_v[...], resid).astype(BF16).reshape(experts, PAD, local)
-    pl.semaphore_wait(near_sem.at[1], 2)
+    heard(2)
     chunk = z // (nz // CHUNKS)
-    for off in reversed(order):
-        for other in (0, 1):
-            if off == 0 and other == 0:
-                continue
-            dst = zdev(off, other)
-            pltpu.make_async_remote_copy(
-                src_ref=out_msg.at[dst],
-                dst_ref=arr.at[ep],
-                send_sem=send_sem.at[2],
-                recv_sem=arr_sem.at[chunk],
-                device_id=(dst, tp),
-                device_id_type=MESH,
-            ).start()
+    out_sem = send_sem.at[2]
+
+    def send(src, dst, sem, other_sem, ring):
+        pltpu.make_async_remote_copy(
+            src_ref=src,
+            dst_ref=dst,
+            send_sem=other_sem,
+            recv_sem=sem,
+            device_id=(ring, tp),
+            device_id_type=MESH,
+        ).start()
+
+    far = (nz // 2 - reach, nz // 2 - 1 - reach)
+    start = (0, 2 * far[0])
+
+    def outbound(way):
+        sign = 1 - 2 * way
+        via = zdev(sign * reach, 0)
+        for i in reversed(range(2 * far[way])):
+            dst = zdev(sign * (reach + i // 2 + 1), i % 2)
+            send(out_msg.at[dst], hand.at[start[way] + i], hand_sem.at[way], out_sem, via)
+        for d in range(reach, 0, -1):
+            for other in (0, 1):
+                dst = zdev(sign * d, other)
+                send(out_msg.at[dst], arr.at[ep], arr_sem.at[chunk], out_sem, dst)
+
+    def hand_on(way):
+        sign = 1 - 2 * way
+        src = zdev(-sign * reach, 0)
+        theirs = arr_sem.at[src // per]
+        arrived(hand.at[pl.ds(start[way], 2 * far[way])], hand_sem.at[way])
+        for i in reversed(range(2 * far[way])):
+            dst = zdev(sign * (i // 2 + 1), i % 2)
+            send(hand.at[start[way] + i], arr.at[src], theirs, send_sem.at[4 + 2 * CHUNKS], dst)
+
+    outbound(0)
+    dst = zdev(0, 1)
+    send(out_msg.at[dst], arr.at[ep], arr_sem.at[chunk], out_sem, dst)
     pltpu.make_async_copy(out_msg.at[ep], arr.at[ep], arr_sem.at[chunk]).start()
+
+    @pl.when(z < reach)
+    def _():
+        pl.semaphore_wait(wrap_sem, reach - z)
+
+    outbound(1)
+    middle = jnp.logical_and(z >= nz // 4, z < nz - nz // 4)
+
+    def hand_on_first(second):
+        @pl.when(middle)
+        def _():
+            hand_on(1 if second else 0)
+
+        @pl.when(jnp.logical_not(middle))
+        def _():
+            hand_on(0 if second else 1)
 
     line, spot = iota((crows, per * PAD), 0), iota((crows, per * PAD), 1)
     compact = ((line % per) * PAD + line // per == spot).astype(BF16)
@@ -370,14 +437,16 @@
         def _():
             pltpu.make_async_copy(back_src.at[ep], back_buf.at[ep], back_sem).start()
 
+    hand_on_first(False)
     gather(0)
+    hand_on_first(True)
+    expert(0, True)
     gather(1)
     gather(2)
-    expert(0, True)
-    expert(2)
+    give_back(0)
     gather(3)
     expert(1)
-    give_back(0)
+    expert(2)
     expert(3)
     give_back(1)
     give_back(2)
@@ -396,6 +465,16 @@
         arrived(rows_buf.at[c, pl.ds(0, others)], send_sem.at[3 + c])
         arrived(down_buf.at[c, pl.ds(0, others)], send_sem.at[3 + CHUNKS + c])
     arrived(back_buf.at[pl.ds(0, experts - 1)], send_sem.at[3 + 2 * CHUNKS])
+    arrived(hand, send_sem.at[4 + 2 * CHUNKS])
+
+
+def write_out(*refs):
+    sems = refs[6]
+    copies = [pltpu.make_async_copy(refs[i], refs[3 + i], sems.at[i]) for i in range(3)]
+    for copy in copies:
+        copy.start()
+    for copy in copies:
+        copy.wait()
 
 
 def local(
@@ -496,18 +575,27 @@
             vmem(experts, PAD, loc),
             vmem(experts, PAD, loc),
             dma((len(operands),)),
-            dma((4 + 2 * CHUNKS,)),
+            dma((5 + 2 * CHUNKS,)),
             dma,
             dma,
             dma((CHUNKS,)),
             dma((CHUNKS,)),
             dma((CHUNKS,)),
             dma,
-            pltpu.SemaphoreType.REGULAR((2,)),
+            pltpu.SemaphoreType.REGULAR((3,)),
+            vmem(4 * (nz // 4) - 2, PAD, loc),
+            dma((2,)),
+            pltpu.SemaphoreType.REGULAR,
         ],
         compiler_params=pltpu.CompilerParams(collective_id=0, has_side_effects=True),
     )(*operands)
-    return made
+    return pl.pallas_call(
+        write_out,
+        out_shape=outs,
+        in_specs=[vmem_spec] * 3,
+        out_specs=(any_spec,) * 3,
+        scratch_shapes=[dma((3,))],
+    )(*[pltpu.with_memory_space_constraint(x, pltpu.VMEM) for x in made])
 
 
 def solution(mesh):

time: 74.2 us -> 71.6 us (0.965)
  local copies, waits for them, and re-layouts: 1.92 us -> 0 us
    unnamed x3 -> x0, local copies, waits for them, and re-layouts: 1.92 us -> none
    pallas_call x1, Pallas kernels: 71.5 us -> 70 us  [local(): pl.pallas_call(functools.partial(kernel, nz, ntp), out_shape=tuple((pltpu...]
where the time goes in v3:
time: 71.6 us; the launch traced here: 71.4 us
  Pallas kernels  70.8 us (99%)
    pallas_call x1, Pallas kernels, local(): pl.pallas_call(functools.partial(kernel, nz, ntp), out_shape=tuple((pltpu...  70 us

profile of v3, /device:TPU:1, one launch (start us, length us, event | category | flops | bytes accessed | tf_op | source)
XLA Modules:
  0.0 71.4 jit_solution(1503500844039214099)
XLA Ops:
  0.6 70.0 %shard_map.229 = (bf16[64,128]{1,0:T(8,128)(2,1)S(1)}, f32[64,4,64]{2,1,0:T(4,128)S(1)}, f32[64,4,64]{2,1,0:T(4,128)S(1)}) custom-call(s32[2,64]{1,0:T(2,128)} %bitcast.30, f32[2,64]{1,0:T(2,128)} %bitcast.31, f32[1,4]{1,0:T(1,128)} %bitcast.32, f32[4,64]{1,0:T(4,128)} %refs_3_.1, f32[4,64]{1,0:T(4,128)} %refs_4_.1, f32[4,16]{1,0:T(4,128)} %refs_5_.1, ...), custom_call_target="tpu_custom_call" | custom-call | tf_op jit(solution)/shard_map/pallas_call | solution.py:552
  70.7 0.7 %shard_map.230 = (bf16[64,128]{1,0:T(8,128)(2,1)}, f32[64,4,64]{2,1,0:T(4,128)}, f32[64,4,64]{2,1,0:T(4,128)}) custom-call(bf16[64,128]{1,0:T(8,128)(2,1)S(1)} %get-tuple-element.6.refs_0_, f32[64,4,64]{2,1,0:T(4,128)S(1)} %get-tuple-element.7.refs_1_, f32[64,4,64]{2,1,0:T(4,128)S(1)} %get-tuple-element.8.refs_2_), custom_call_target="tpu_custom_call" | custom-call | tf_op jit(solution)/shard_map/pallas_call | solution.py:592
